TPU v7x, 512 devices: a whole 4x4x16 slice. The times are simulated.
512 devices in a mesh: sp: 16 (over y, x), tp: 32 (over z, core).
Axes of the slice: x: 4, y: 4, z: 16, core: 2. Of those that a mesh axis runs over, the one named last changes fastest.
Arguments:
- tokens: bfloat16 [3, 8192, 4096], P(None, 'sp', 'tp'), may hold values from -6 to 6
- new_token: bfloat16 [3, 1, 4096], P(None, None, 'tp'), may hold values from -6 to 6
- query_weight: bfloat16 [4096, 4096], P(None, 'tp'), may hold values from -0.09375 to 0.09375
- key_weight: bfloat16 [4096, 4096], P(None, 'tp'), may hold values from -0.09375 to 0.09375
- value_weight: bfloat16 [4096, 4096], P(None, 'tp'), may hold values from -0.09375 to 0.09375
- log_decay: float32 [64], P('tp'), may hold values from -0.034 to 0
Outputs:
- state: bfloat16 [3, 64, 64, 64], P(None, 'tp', 'sp')
- read: bfloat16 [3, 4096], P(None, 'tp')
All inputs are finite; a program needn't handle non-finite values.
Results may differ from a plain program's by a relative error of at most 0.012.
Values may be sent and summed in bfloat16 or wider, within the bound.
No kernel may reach another device: no remote copies, remote signals or barrier semaphores. Data moves between devices by JAX's collectives and lax.ppermute only.
A program may use at most 64 MiB of HBM per device.

v0:
```python
import jax
import jax.numpy as jnp
from jax import lax
from jax.sharding import PartitionSpec as P

HD = 64


def cut_along(value, dim, count):
    dims = value.shape
    tiles = value.reshape(*dims[:dim], count, dims[dim] // count, *dims[dim + 1 :])
    return jnp.moveaxis(tiles, dim, 0)


def sent_and_summed(value, axis, dim):
    tiles = cut_along(value, dim, lax.axis_size(axis))
    arrived = lax.all_to_all(tiles, axis, split_axis=0, concat_axis=0, tiled=True)
    return arrived.sum(axis=0)


def from_everyone(value, axis):
    copies = jnp.broadcast_to(value, (lax.axis_size(axis), *value.shape))
    return lax.all_to_all(copies, axis, split_axis=0, concat_axis=0, tiled=True)


def over_copies(value, axis):
    everything = from_everyone(value, axis)
    return jnp.sum(everything, axis=0)


def rotate(values, positions):
    half_dim = values.shape[-1] // 2
    inverse = 10000.0 ** (-jnp.arange(half_dim, dtype=jnp.float32) / half_dim)
    angles = positions.astype(jnp.float32)[:, None, None] * inverse[None, None, :]
    cosine = jnp.cos(angles)
    sine_part = jnp.sin(angles)
    first = values[..., :half_dim]
    second = values[..., half_dim:]
    return jnp.concatenate(
        [first * cosine - second * sine_part, first * sine_part + second * cosine], axis=-1
    )


def group_norm(output):
    centered = output - jnp.mean(output, axis=-1, keepdims=True)
    return centered * lax.rsqrt(jnp.mean(centered * centered, axis=-1, keepdims=True) + 1e-05)


def body(tokens, new_token, query_weight, key_weight, value_weight, log_decay):
    sequences, span_len, _ = tokens.shape
    head_count = log_decay.shape[0]
    inner = head_count * HD
    groups = lax.axis_size("sp")
    own_index = lax.axis_index("sp")
    key_scale = HD ** (-0.5)
    row_weights = jnp.concatenate([key_weight, value_weight], axis=1)
    all_weights = jnp.concatenate([key_weight, value_weight, query_weight], axis=1)
    row_piece = lax.all_gather(tokens, "tp", axis=2, tiled=True)
    new_piece = lax.all_gather(new_token, "tp", axis=2, tiled=True)
    row_total = jnp.dot(row_piece, row_weights, preferred_element_type=jnp.float32)
    new_total = jnp.dot(new_piece, all_weights, preferred_element_type=jnp.float32)
    row_total = row_total.reshape(sequences, span_len, 2, head_count, HD)
    offsets = own_index * span_len + jnp.arange(span_len, dtype=jnp.int32)
    key_rows = (rotate(row_total[:, :, 0], offsets) * key_scale).astype(jnp.bfloat16)
    value_rows = row_total[:, :, 1].astype(jnp.bfloat16)
    to_end = (span_len - 1 - jnp.arange(span_len, dtype=jnp.int32)).astype(jnp.float32)
    decay_rows = jnp.exp(to_end[:, None] * log_decay[None, :])
    weighted = (key_rows.astype(jnp.float32) * decay_rows[None, :, :, None]).astype(jnp.bfloat16)
    span_state = jnp.einsum(
        "sthk,sthv->shkv", weighted, value_rows, preferred_element_type=jnp.float32
    )
    carried_state = jnp.exp(log_decay * (span_len * (groups - 1 - own_index)).astype(jnp.float32))
    scaled_state = span_state * carried_state[None, :, None, None]
    state_rows = sent_and_summed(scaled_state, "sp", 2)
    new_total = new_total.reshape(sequences, 1, 3, head_count, HD)
    new_position = jnp.full((1,), groups * span_len, jnp.int32)
    fresh_key = (rotate(new_total[:, :, 0], new_position) * key_scale).astype(jnp.bfloat16)[:, 0]
    new_value = new_total[:, 0, 1].astype(jnp.bfloat16)
    new_query = rotate(new_total[:, :, 2], new_position).astype(jnp.bfloat16)[:, 0]
    query_entries = new_query.astype(jnp.float32)
    decay_one = jnp.exp(log_decay)[None, :, None]
    partial_read = (
        jnp.einsum("shkv,shk->shv", scaled_state, query_entries, precision=lax.Precision.HIGHEST)
        * decay_one
    )
    summed = over_copies(partial_read, "sp")
    own_term = jnp.sum(
        query_entries * fresh_key.astype(jnp.float32), axis=-1, keepdims=True
    ) * new_value.astype(jnp.float32)
    normed = group_norm(summed + own_term)
    return (state_rows.astype(jnp.bfloat16), normed.reshape(sequences, inner).astype(jnp.bfloat16))


def solution(mesh):
    return jax.shard_map(
        body,
        mesh=mesh,
        in_specs=(
            P(None, "sp", "tp"),
            P(None, None, "tp"),
            P(None, "tp"),
            P(None, "tp"),
            P(None, "tp"),
            P("tp"),
        ),
        out_specs=(P(None, "tp", "sp", None), P(None, "tp")),
        check_vma=False,
    )
```

profile of v0, /device:TPU:32, one launch (start us, length us, event | category | flops | bytes accessed | tf_op | source)
XLA Modules:
  0.0 172.4 jit_solution(1786247637780565341)
XLA Ops:
  7.2 0.0 copy-start
  7.2 0.0 copy-start.1
  7.2 0.0 copy-start.3
  7.2 0.0 all-gather.2.cloned.1.call-start
  7.2 0.7 all-gather.2.cloned.1.call-update
  7.9 1.5 copy.27
  9.4 0.0 copy-done.1
  9.4 1.4 copy.26
  10.8 34.3 %all_gather.7 = bf16[3,1,4096]{2,0,1:T(4,128)(2,1)S(1)} all-gather(bf16[3,1,128]{2,0,1:T(4,128)(2,1)S(1)} %copy-done.3), channel_id=1, replica_groups=mesh['sp'=16,'tp'=32] {'tp'}, dimensions={2}, use_global_device_ids=true | all-gather | bytes 25344 | tf_op jit(solution)/shard_map/all_gather | solution.py:59
  45.1 0.0 copy-done
  45.1 1.9 %fusion.9 = f32[3,384]{1,0:T(4,128)S(1)} fusion(bf16[4096,128]{1,0:T(8,128)(2,1)} %param.8, bf16[4096,128]{1,0:T(8,128)(2,1)S(1)} %copy-done, bf16[4096,128]{1,0:T(8,128)(2,1)S(1)} %copy-done.1, bf16[3,1,4096]{2,0,1:T(4,128)(2,1)S(1)} %all_gather.7), kind=kOutput, calls=%fused_computation.11 | convolution fusion | flops 18874368 | bytes 3174912 | tf_op jit(solution)/shard_map/dot_general | solution.py:61
  47.0 0.1 reshape.207
  47.1 0.1 multiply_sine_fusion.1
  47.1 0.1 subtract_bitcast_fusion
  47.2 0.1 fusion.31
  47.3 0.1 multiply_exponential_fusion
  47.4 0.3 multiply_cosine_fusion
  47.7 82.5 %all-gather.2.cloned.1.call-done = bf16[3,512,4096]{2,1,0:T(8,128)(2,1)} async-done(((bf16[3,512,128]{2,1,0:T(8,128)(2,1)}), bf16[3,512,4096]{2,1,0:T(8,128)(2,1)}) %all-gather.2.cloned.1.call-update) | async-done | bytes 12582928 | tf_op jit(solution)/shard_map/all_gather | solution.py:58
  130.3 6.8 %fusion.6 = f32[256,3,512]{2,0,1:T(8,128)S(1)} fusion(bf16[3,512,4096]{2,1,0:T(8,128)(2,1)} %all-gather.2.cloned.1.call-done, bf16[4096,128]{0,1:T(8,128)(2,1)S(1)} %copy.27, bf16[4096,128]{0,1:T(8,128)(2,1)} %copy.26), kind=kOutput, calls=%fused_computation.7 | convolution fusion | flops 3225419776 | bytes 16252928 | tf_op jit(solution)/shard_map/dot_general | solution.py:60
  137.0 0.1 copy_bitcast_fusion
  137.1 0.1 multiply_subtract_fusion
  137.2 0.3 convolution_multiply_fusion
  137.5 0.2 fusion.22
  137.7 0.1 broadcast_multiply_fusion
  137.8 0.7 reshape.215
  138.5 6.4 %all-to-all-start.1 = ((f32[16,1,384]{2,1,0:T(1,128)}), f32[16,1,384]{2,1,0:T(1,128)S(1)}, u32[]{:S(2)}, u32[]{:S(2)}) async-start(f32[16,1,384]{2,1,0:T(1,128)} %reshape.215), calls=%async_computation.1 | async-start | bytes 49152 | tf_op jit(solution)/shard_map/all_to_all | solution.py:23
  145.0 0.2 multiply_reduce_fusion.1
  145.1 0.1 mul.279
  145.2 0.1 mul.280
  145.3 0.1 reshape.208
  145.4 0.8 reshape.213
  146.2 6.3 %all-to-all-done.1 = f32[16,1,384]{2,1,0:T(1,128)S(1)} async-done(((f32[16,1,384]{2,1,0:T(1,128)}), f32[16,1,384]{2,1,0:T(1,128)S(1)}, u32[]{:S(2)}, u32[]{:S(2)}) %all-to-all-start.1) | async-done | bytes 24608 | tf_op jit(solution)/shard_map/all_to_all | solution.py:23
  152.5 3.5 %all-to-all-start = ((f32[16,1,1536]{2,1,0:T(1,128)}), f32[16,1,1536]{2,1,0:T(1,128)S(1)}, u32[]{:S(2)}, u32[]{:S(2)}) async-start(f32[16,1,1536]{2,1,0:T(1,128)} %reshape.213), calls=%async_computation | async-start | bytes 196608 | tf_op jit(solution)/shard_map/all_to_all | solution.py:17
  156.1 0.5 broadcast.164
  156.6 0.7 reduce.1
  157.3 0.1 reshape.216
  157.4 0.2 fusion.32
  157.6 0.1 reduce_sum.49
  157.7 0.2 multiply_reduce_fusion
  157.8 0.1 mul.284
  157.9 0.1 mul.285
  158.0 0.1 sub.41
  158.1 0.1 sub.42
  158.2 0.6 multiply_convert_fusion.2
  158.7 5.1 %all-to-all-done = f32[16,1,1536]{2,1,0:T(1,128)S(1)} async-done(((f32[16,1,1536]{2,1,0:T(1,128)}), f32[16,1,1536]{2,1,0:T(1,128)S(1)}, u32[]{:S(2)}, u32[]{:S(2)}) %all-to-all-start) | async-done | bytes 98336 | tf_op jit(solution)/shard_map/all_to_all | solution.py:17
  163.8 0.9 reduce
  164.7 0.1 reshape.214
  164.9 0.7 reduce_sum.47
  (14 shorter events, 0.2 us)
Async XLA Ops:
  7.2 37.9 %copy-start = (bf16[4096,128]{1,0:T(8,128)(2,1)S(1)}, bf16[4096,128]{1,0:T(8,128)(2,1)}, u32[]{:S(2)}) copy-start(bf16[4096,128]{1,0:T(8,128)(2,1)} %param.10) | copy-start | bytes 3145732
  7.2 2.3 %copy-start.1 = (bf16[4096,128]{1,0:T(8,128)(2,1)S(1)}, bf16[4096,128]{1,0:T(8,128)(2,1)}, u32[]{:S(2)}) copy-start(bf16[4096,128]{1,0:T(8,128)(2,1)} %param.9) | copy-start | bytes 3145732
  7.2 3.6 %copy-start.3 = (bf16[3,1,128]{2,0,1:T(4,128)(2,1)S(1)}, bf16[3,1,128]{2,0,1:T(4,128)(2,1)}, u32[]{:S(2)}) copy-start(bf16[3,1,128]{2,0,1:T(4,128)(2,1)} %param.7) | copy-start | bytes 2308
  7.2 123.1 %all-gather.2.cloned.1.call-start = ((), (), s32[]{:S(2)}) async-start(), calls=%async_computation.2 | async-start | bytes 12976128 | tf_op jit(solution)/shard_map/all_gather | solution.py:58
  45.1 2.3 %copy-start.2 = (f32[2]{0:T(128)S(1)}, f32[2]{0:T(128)}, u32[]{:S(2)}) copy-start(f32[2]{0:T(128)} %param.11) | copy-start | bytes 28
  138.5 14.0 %all-to-all-start.1 = ((f32[16,1,384]{2,1,0:T(1,128)}), f32[16,1,384]{2,1,0:T(1,128)S(1)}, u32[]{:S(2)}, u32[]{:S(2)}) async-start(f32[16,1,384]{2,1,0:T(1,128)} %reshape.215), calls=%async_computation.1 | async-start | bytes 49152 | tf_op jit(solution)/shard_map/all_to_all | solution.py:23
  152.5 11.3 %all-to-all-start = ((f32[16,1,1536]{2,1,0:T(1,128)}), f32[16,1,1536]{2,1,0:T(1,128)S(1)}, u32[]{:S(2)}, u32[]{:S(2)}) async-start(f32[16,1,1536]{2,1,0:T(1,128)} %reshape.213), calls=%async_computation | async-start | bytes 196608 | tf_op jit(solution)/shard_map/all_to_all | solution.py:17
Sparse Core Ops, SparseCore 0:
  10.0 120.1 all-gather.1
where the time goes:
time: 173 us; the launch traced here: 172 us
  waiting for transfers between devices  94.6 us (55%)
  blocking collectives  34.3 us (20%)
  between operations  14.2 us (8%)
  starting transfers between devices  9.96 us (6%)
  matrix products  9.15 us (5%)
  local copies, waits for them, and re-layouts  5.97 us (3%)
  other arithmetic  4.17 us (2%)
    all_gather x1, waiting for transfers between devices, body(): row_piece = lax.all_gather(tokens, 'tp', axis=2, tiled=True)  82.5 us
    all_gather x1, blocking collectives, body(): new_piece = lax.all_gather(new_token, 'tp', axis=2, tiled=True)  34.3 us
    dot_general x1, matrix products, body(): jnp.dot(row_piece, row_weights, preferred_element_type=jnp.float32)  6.76 us
    all_to_all x1, starting transfers between devices, from_everyone(): return lax.all_to_all(copies, axis, split_axis=0, concat_axis=0, tiled=True)  6.41 us
    all_to_all x1, waiting for transfers between devices, from_everyone(): return lax.all_to_all(copies, axis, split_axis=0, concat_axis=0, tiled=True)  6.33 us
    all_to_all x1, waiting for transfers between devices, sent_and_summed(): lax.all_to_all(tiles, axis, split_axis=0, concat_axis=0, tiled=True)  5.1 us
    unnamed x14, local copies, waits for them, and re-layouts  4.6 us
    all_to_all x1, starting transfers between devices, sent_and_summed(): lax.all_to_all(tiles, axis, split_axis=0, concat_axis=0, tiled=True)  3.51 us
  transfers between devices with their start and end apart: 3, of which 3 were waited for; matrix products, arithmetic and copies ran while one was open for 5% of the time, Pallas kernels for 0%

commit v1 on v0

--- a/solution.py
+++ b/solution.py
@@ -55,7 +55,17 @@
     key_scale = HD ** (-0.5)
     row_weights = jnp.concatenate([key_weight, value_weight], axis=1)
     all_weights = jnp.concatenate([key_weight, value_weight, query_weight], axis=1)
-    row_piece = lax.all_gather(tokens, "tp", axis=2, tiled=True)
+
+    def track_the_heaps(row_data, row_axis):
+        ready = jnp.concatenate(
+            lax.all_to_all(
+                jnp.stack([row_data for _ in range(lax.axis_size(row_axis))], 0), row_axis, 0, 0
+            ),
+            2,
+        )
+        return ready
+
+    row_piece = track_the_heaps(tokens, "tp")
     new_piece = lax.all_gather(new_token, "tp", axis=2, tiled=True)
     row_total = jnp.dot(row_piece, row_weights, preferred_element_type=jnp.float32)
     new_total = jnp.dot(new_piece, all_weights, preferred_element_type=jnp.float32)

time: 173 us -> 629 us (3.64)
  the two profiles are of different devices: /device:TPU:32 before, /device:TPU:2 now
where the time goes in v1:
time: 629 us; the launch traced here: 628 us
  blocking collectives  564 us (90%)
  starting transfers between devices  28 us (4%)
  local copies, waits for them, and re-layouts  13.6 us (2%)
  matrix products  9.02 us (1%)
  waiting for transfers between devices  8.85 us (1%)
    all_gather x1, blocking collectives, body(): new_piece = lax.all_gather(new_token, 'tp', axis=2, tiled=True)  564 us
    all_to_all x1, starting transfers between devices, track_the_heaps(): lax.all_to_all(jnp.stack([row_data for _ in range(lax.axis_size(row_axis)...  15.7 us
  transfers between devices with their start and end apart: 3, of which 2 were waited for; matrix products, arithmetic and copies ran while one was open for 1% of the time, Pallas kernels for 0%

profile of v1, /device:TPU:2, one launch (start us, length us, event | category | flops | bytes accessed | tf_op | source)
XLA Modules:
  0.0 628.1 jit_solution(14454574913981206434)
XLA Ops:
  0.6 8.6 %stack.2 = bf16[32,3,512,128]{3,2,1,0:T(8,128)(2,1)} broadcast(bf16[3,512,128]{2,1,0:T(8,128)(2,1)} %param.6), dimensions={1,2,3} | broadcast | bytes 12976128 | tf_op jit(solution)/shard_map/stack | solution.py:62
  9.2 15.7 %all-to-all-start = ((bf16[32,3,512,128]{3,2,1,0:T(8,128)(2,1)}), bf16[32,3,512,128]{3,2,1,0:T(8,128)(2,1)}, u32[]{:S(2)}, u32[]{:S(2)}) async-start(bf16[32,3,512,128]{3,2,1,0:T(8,128)(2,1)} %stack.2), calls=%async_computation | async-start | bytes 25165824 | tf_op jit(solution)/shard_map/all_to_all | solution.py:61
  25.0 0.0 copy-start.3
  25.0 0.0 copy-done.1
  25.0 0.5 copy.28
  25.5 0.0 copy-done
  25.5 1.4 copy.29
  26.9 0.0 copy-done.3
  26.9 563.7 %all_gather.3 = bf16[3,1,4096]{2,0,1:T(4,128)(2,1)S(1)} all-gather(bf16[3,1,128]{2,0,1:T(4,128)(2,1)S(1)} %copy-done.3), channel_id=1, replica_groups=mesh['sp'=16,'tp'=32] {'tp'}, dimensions={2}, use_global_device_ids=true | all-gather | bytes 25344 | tf_op jit(solution)/shard_map/all_gather | solution.py:69
  590.6 1.7 fusion.11
  592.4 0.1 reshape.217
  592.5 0.1 multiply_sine_fusion.1
  592.5 0.1 subtract_bitcast_fusion
  592.6 0.1 fusion.33
  592.7 0.0 copy-done.2
  592.7 0.1 multiply_exponential_fusion
  592.8 0.3 multiply_cosine_fusion
  593.1 0.0 all-to-all-done
  593.1 6.8 %fusion = f32[256,3,512]{2,0,1:T(8,128)S(1)} fusion(bf16[4096,128]{0,1:T(8,128)(2,1)} %copy.29, bf16[4096,128]{0,1:T(8,128)(2,1)S(1)} %copy.28, bf16[32,3,512,128]{3,2,1,0:T(8,128)(2,1)} %all-to-all-done), kind=kOutput, calls=%fused_computation | convolution fusion | flops 3225419776 | bytes 16252928 | tf_op jit(solution)/shard_map/dot_general | solution.py:70
  600.0 0.1 copy_bitcast_fusion
  600.0 0.1 multiply_subtract_fusion
  600.2 0.3 convolution_multiply_fusion
  600.4 0.2 fusion.24
  600.6 0.1 broadcast_multiply_fusion
  600.8 0.7 reshape.225
  601.5 7.5 %all-to-all-start.2 = ((f32[16,1,384]{2,1,0:T(1,128)}), f32[16,1,384]{2,1,0:T(1,128)S(1)}, u32[]{:S(2)}, u32[]{:S(2)}) async-start(f32[16,1,384]{2,1,0:T(1,128)} %reshape.225), calls=%async_computation.2 | async-start | bytes 49152 | tf_op jit(solution)/shard_map/all_to_all | solution.py:23
  608.9 0.2 multiply_reduce_fusion.1
  609.1 0.1 mul.279
  609.2 0.1 mul.280
  609.3 0.1 reshape.218
  609.4 0.8 reshape.223
  610.2 5.0 all-to-all-done.2
  615.2 4.8 all-to-all-start.1
  619.9 0.5 broadcast.166
  620.4 0.7 reduce.1
  621.2 0.1 reshape.226
  621.3 0.2 fusion.34
  621.5 0.1 reduce_sum.49
  621.5 0.2 multiply_reduce_fusion
  621.7 0.1 mul.284
  621.8 0.1 mul.285
  621.9 0.1 sub.41
  621.9 0.1 sub.42
  622.0 0.6 multiply_convert_fusion.2
  622.6 3.9 all-to-all-done.1
  626.5 0.9 reduce
  627.4 0.1 reshape.224
  627.5 0.7 reduce_sum.47
  (14 shorter events, 0.2 us)
Async XLA Ops:
  9.2 15.8 %copy-start.1 = (bf16[4096,128]{1,0:T(8,128)(2,1)S(1)}, bf16[4096,128]{1,0:T(8,128)(2,1)}, u32[]{:S(2)}) copy-start(bf16[4096,128]{1,0:T(8,128)(2,1)} %param.9) | copy-start | bytes 3145732
  9.2 16.3 %copy-start = (bf16[4096,128]{1,0:T(8,128)(2,1)S(1)}, bf16[4096,128]{1,0:T(8,128)(2,1)}, u32[]{:S(2)}) copy-start(bf16[4096,128]{1,0:T(8,128)(2,1)} %param.10) | copy-start | bytes 3145732
  9.2 583.9 %all-to-all-start = ((bf16[32,3,512,128]{3,2,1,0:T(8,128)(2,1)}), bf16[32,3,512,128]{3,2,1,0:T(8,128)(2,1)}, u32[]{:S(2)}, u32[]{:S(2)}) async-start(bf16[32,3,512,128]{3,2,1,0:T(8,128)(2,1)} %stack.2), calls=%async_computation | async-start | bytes 25165824 | tf_op jit(solution)/shard_map/all_to_all | solution.py:61
  25.0 1.9 copy-start.3
  590.6 2.1 copy-start.2
  601.5 13.7 %all-to-all-start.2 = ((f32[16,1,384]{2,1,0:T(1,128)}), f32[16,1,384]{2,1,0:T(1,128)S(1)}, u32[]{:S(2)}, u32[]{:S(2)}) async-start(f32[16,1,384]{2,1,0:T(1,128)} %reshape.225), calls=%async_computation.2 | async-start | bytes 49152 | tf_op jit(solution)/shard_map/all_to_all | solution.py:23
  615.2 11.3 %all-to-all-start.1 = ((f32[16,1,1536]{2,1,0:T(1,128)}), f32[16,1,1536]{2,1,0:T(1,128)S(1)}, u32[]{:S(2)}, u32[]{:S(2)}) async-start(f32[16,1,1536]{2,1,0:T(1,128)} %reshape.223), calls=%async_computation.1 | async-start | bytes 196608 | tf_op jit(solution)/shard_map/all_to_all | solution.py:17
